TPU v7x, 32 devices: a whole 2x2x4 slice. The times are simulated.
32 devices in a mesh: ep: 8 (over z, x), tp: 4 (over y, core).
Axes of the slice: x: 2, y: 2, z: 4, core: 2. Of those that a mesh axis runs over, the one named last changes fastest.
Arguments:
- tokens: bfloat16 [2048, 4096], P('ep', 'tp'), may hold values from -540 to 540
- norm_gain: float32 [4096], P('tp'), may hold values from 0.1 to 1.9
- expert_ids: int32 [2048, 2], P('ep'), may hold values from 0 to 7, all different within a row; in each aligned block of 256 rows (0 to 255, 256 to 511, ...) at most 96 rows name the same one
- expert_weights: float32 [2048, 2], P('ep'), may hold values from 0.1 to 1
- gate_weight: bfloat16 [8, 4096, 2048], P('ep', None, 'tp'), may hold values from -0.09375 to 0.09375
- up_weight: bfloat16 [8, 4096, 2048], P('ep', None, 'tp'), may hold values from -0.09375 to 0.09375
- down_weight: bfloat16 [8, 2048, 4096], P('ep', None, 'tp'), may hold values from -0.125 to 0.125
Outputs:
- mixed: bfloat16 [2048, 4096], P('ep', 'tp')
Inputs may be any that keep to these rules, and one draw needn't show every extreme that they name: `expert_ids`: each row names 2 different experts. Among the rows of one index of ep, no expert is named by more than 96 rows, a bound that some block reaches.
All inputs are finite; a program needn't handle non-finite values.
Results may differ from a plain program's by a relative error of at most 0.007.
Values may be sent and summed in bfloat16 or wider, within the bound.
A program may use at most 64 MiB of HBM per device.

v0:
```python
import functools

import jax
import jax.numpy as jnp
from jax import lax
from jax.experimental import pallas as pl
from jax.experimental.pallas import tpu as pltpu
from jax.sharding import PartitionSpec as P

MESH = pl.DeviceIdType.MESH
F32 = jnp.float32
BF16 = jnp.bfloat16


def kernel(
    n_ep, n_tp, groups, cap,
    tok, gain, ids, wts, gate_hbm, up_hbm, down_hbm,
    out,
    wg, wu, wd, squares_out, squares_in, key, weight, outgoing, rows, hid, prod, ret, acc,
    w_sem, sq_send, sq_recv, d_send, d_recv, ry_send, rp_send, r_recv,
    hy_send, hp_send, h_recv, b_send, b_recv,
):
    e = lax.axis_index("ep")
    t = lax.axis_index("tp")
    size = n_ep // groups
    block, place = e // size, e % size
    n_tok, width = tok.shape
    partner = t + 1 - 2 * (t % 2)
    pairs = n_tp // 2

    loads = [
        pltpu.make_async_copy(gate_hbm.at[0], wg, w_sem.at[0]),
        pltpu.make_async_copy(up_hbm.at[0], wu, w_sem.at[1]),
        pltpu.make_async_copy(down_hbm.at[0], wd, w_sem.at[2]),
    ]
    for load in loads:
        load.start()

    barrier = pltpu.get_barrier_semaphore()
    for i in range(1, n_ep):
        pl.semaphore_signal(barrier, inc=1, device_id={"ep": (e + i) % n_ep}, device_id_type=MESH)
    for i in range(1, n_tp):
        pl.semaphore_signal(barrier, inc=1, device_id={"tp": (t + i) % n_tp}, device_id_type=MESH)

    x = tok[...].astype(F32)
    part = jnp.sum(x * x, axis=1, keepdims=True)
    part = jnp.transpose(jnp.broadcast_to(part, (n_tok, 128)))[0:8]
    squares_out[...] = part
    pl.semaphore_wait(barrier, n_ep + n_tp - 2)

    def sq_copy(i, shard):
        return pltpu.make_async_remote_copy(
            squares_out, squares_in.at[shard], sq_send.at[i], sq_recv.at[shard],
            device_id={"tp": (t + i) % n_tp}, device_id_type=MESH)

    for i in range(1, n_tp):
        sq_copy(i, t).start()

    experts = key.shape[0]
    which = lax.broadcasted_iota(jnp.int32, (experts, n_tok), 0)
    first, second = ids[0:1, :] == which, ids[1:2, :] == which
    named = jnp.where(first | second, 1.0, 0.0)
    before = lax.broadcasted_iota(jnp.int32, (n_tok, n_tok), 0) < lax.broadcasted_iota(
        jnp.int32, (n_tok, n_tok), 1)
    rank = jnp.dot(named.astype(BF16), jnp.where(before, 1.0, 0.0).astype(BF16),
                   preferred_element_type=F32)
    slot = jnp.where(first | second, rank, -1.0)
    share = jnp.where(first, wts[0:1, :], 0.0) + jnp.where(second, wts[1:2, :], 0.0)
    for d in range(experts):
        key[d] = jnp.broadcast_to(slot[d:d + 1], (8, n_tok))
        weight[d] = jnp.broadcast_to(share[d:d + 1], (8, n_tok))
    number = (lax.broadcasted_iota(jnp.int32, (cap // 8, 8, n_tok), 0) * 8
              + lax.broadcasted_iota(jnp.int32, (cap // 8, 8, n_tok), 1)).astype(F32)

    def chosen(d, value):
        return jnp.where(number == key[d][None], value, 0.0).reshape(cap, n_tok)

    total = part
    for i in range(1, n_tp):
        other = (t + i) % n_tp
        sq_copy(i, other).wait_recv()
        total = total + squares_in[other]
    inv = lax.rsqrt(total / (width * n_tp) + 1e-06)
    inv = jnp.transpose(jnp.broadcast_to(inv[0:1], (128, n_tok)))[:, 0:1]
    normed = (tok[...].astype(F32) * inv * gain[...]).astype(BF16)

    def member(k, j):
        return (block ^ k) * size + (place + j) % size

    def dispatch(d, s):
        return pltpu.make_async_remote_copy(
            outgoing.at[d], rows.at[t, s], d_send.at[d], d_recv.at[s],
            device_id={"ep": d}, device_id_type=MESH)

    def back(s, d):
        return pltpu.make_async_remote_copy(
            prod.at[s], ret.at[d], b_send.at[s], b_recv.at[d],
            device_id={"ep": s}, device_id_type=MESH)

    def peers(k):
        return range(1 if k == 0 else 0, size)

    def picked(d):
        return jnp.dot(chosen(d, 1.0).astype(BF16), normed,
                       preferred_element_type=F32).astype(BF16)

    for k in range(groups):
        for j in peers(k):
            d = member(k, j)
            outgoing[d] = picked(d)
            dispatch(d, e).start()
    rows[t, e] = picked(e)

    def span(k):
        return pl.ds((block ^ k) * size, size)

    def across(buf, k, i, shard, send, recv):
        ref = buf.at[shard, span(k)]
        return pltpu.make_async_remote_copy(
            ref, ref, send.at[i, k], recv.at[shard, k],
            device_id={"tp": (t + 2 * i) % n_tp}, device_id_type=MESH)

    def beside(buf, k, i, shard, send, recv):
        ref = buf.at[shard, span(k)]
        return pltpu.make_async_remote_copy(
            ref, ref, send.at[i, k], recv.at[shard, k],
            device_id={"tp": partner}, device_id_type=MESH)

    def spread(buf, k, ysend, psend, recv):
        for i in range(1, pairs):
            across(buf, k, i, t, ysend, recv).start()
        beside(buf, k, 0, t, psend, recv).start()

    def pass_on(buf, k, ysend, psend, recv):
        for i in range(1, pairs):
            shard = (t + n_tp - 2 * i) % n_tp
            across(buf, k, i, shard, ysend, recv).wait_recv()
            beside(buf, k, i, shard, psend, recv).start()

    def complete(buf, k, psend, recv):
        for i in range(pairs):
            shard = (partner + n_tp - 2 * i) % n_tp
            beside(buf, k, i, shard, psend, recv).wait_recv()

    row_sems, hid_sems = (ry_send, rp_send, r_recv), (hy_send, hp_send, h_recv)

    def stage_a(k):
        for j in peers(k):
            s = member(k, j)
            dispatch(s, s).wait_recv()
        spread(rows, k, *row_sems)

    def stage_b(k):
        pass_on(rows, k, *row_sems)

    def stage_c(k):
        complete(rows, k, rp_send, r_recv)
        if k == 0:
            loads[0].wait()
            loads[1].wait()
        gate = up = None
        for shard in range(n_tp):
            part_rows = rows[shard, span(k)].reshape(size * cap, width)
            g = jnp.dot(part_rows, wg[shard * width:(shard + 1) * width, :],
                        preferred_element_type=F32)
            u = jnp.dot(part_rows, wu[shard * width:(shard + 1) * width, :],
                        preferred_element_type=F32)
            gate, up = (g, u) if gate is None else (gate + g, up + u)
        hidden = (gate / (1.0 + jnp.exp(-gate)) * up).astype(BF16)
        hid[t, span(k)] = hidden.reshape(size, cap, hidden.shape[1])
        spread(hid, k, *hid_sems)

    def stage_d(k):
        pass_on(hid, k, *hid_sems)

    def stage_e(k):
        complete(hid, k, hp_send, h_recv)
        if k == 0:
            loads[2].wait()
        units = hid.shape[3]
        made = None
        for shard in range(n_tp):
            m = jnp.dot(hid[shard, span(k)].reshape(size * cap, units),
                        wd[shard * units:(shard + 1) * units, :], preferred_element_type=F32)
            made = m if made is None else made + m
        prod[span(k)] = made.astype(BF16).reshape(size, cap, width)
        for j in peers(k):
            back(member(k, j), e).start()
        if k == 0:
            ret[e] = prod[e]

    def stage_f(k):
        for j in peers(k):
            d = member(k, j)
            back(d, d).wait_recv()
        tables = jnp.concatenate(
            [chosen((block ^ k) * size + j, weight[(block ^ k) * size + j][None])
             for j in range(size)], axis=0)
        high = tables.astype(BF16)
        low = (tables - high.astype(F32)).astype(BF16)
        values = ret[span(k)].reshape(size * cap, width)
        dims = (((0,), (0,)), ((), ()))
        sums = lax.dot_general(high, values, dims, preferred_element_type=F32)
        sums = sums + lax.dot_general(low, values, dims, preferred_element_type=F32)
        if k > 0:
            sums = sums + acc[...]
        if k < groups - 1:
            acc[...] = sums
        else:
            out[...] = sums.astype(BF16)

    stages = dict(a=stage_a, b=stage_b, c=stage_c, d=stage_d, e=stage_e, f=stage_f)
    order, lead = [], min(2, groups)
    for k in range(lead):
        order.append(("a", k))
    for k in range(groups):
        if k + lead < groups:
            order.append(("a", k + lead))
        order += [("b", k), ("c", k)]
        if k > 0:
            order += [("d", k - 1), ("e", k - 1)]
    last = groups - 1
    order += [("f", k) for k in range(last - 2)]
    order += [("d", last), ("e", last)]
    order += [("f", k) for k in range(max(0, last - 2), groups)]
    for name, k in order:
        stages[name](k)

    for i in range(1, n_tp):
        sq_copy(i, t).wait_send()
    for k in range(groups):
        for j in peers(k):
            d = member(k, j)
            dispatch(d, e).wait_send()
            back(d, e).wait_send()
        for buf, ysend, psend, recv in ((rows,) + row_sems, (hid,) + hid_sems):
            for i in range(pairs):
                if i > 0:
                    across(buf, k, i, t, ysend, recv).wait_send()
                beside(buf, k, i, t, psend, recv).wait_send()


def body(n_ep, n_tp, tokens, norm_gain, expert_ids, expert_weights, gate_weight, up_weight, down_weight):
    n_tok, width = tokens.shape
    experts = gate_weight.shape[0] * n_ep
    cap = 3 * n_tok * expert_ids.shape[1] // (2 * experts)
    depth, units = gate_weight.shape[1:]
    hidden = down_weight.shape[1]
    groups = next(g for g in (8, 4, 2, 1) if n_ep % g == 0)
    vmem = pl.BlockSpec(memory_space=pltpu.VMEM)
    hbm = pl.BlockSpec(memory_space=pl.ANY)
    dma = pltpu.SemaphoreType.DMA
    return pl.pallas_call(
        functools.partial(kernel, n_ep, n_tp, groups, cap),
        out_shape=jax.ShapeDtypeStruct((n_tok, width), BF16),
        in_specs=[vmem] * 4 + [hbm] * 3,
        out_specs=vmem,
        scratch_shapes=[
            pltpu.VMEM((depth, units), BF16),
            pltpu.VMEM((depth, units), BF16),
            pltpu.VMEM((hidden, width), BF16),
            pltpu.VMEM((8, n_tok), F32),
            pltpu.VMEM((n_tp, 8, n_tok), F32),
            pltpu.VMEM((experts, 8, n_tok), F32),
            pltpu.VMEM((experts, 8, n_tok), F32),
            pltpu.VMEM((n_ep, cap, width), BF16),
            pltpu.VMEM((n_tp, n_ep, cap, width), BF16),
            pltpu.VMEM((n_tp, n_ep, cap, units), BF16),
            pltpu.VMEM((n_ep, cap, width), BF16),
            pltpu.VMEM((n_ep, cap, width), BF16),
            pltpu.VMEM((n_tok, width), F32),
            dma((3,)), dma((n_tp,)), dma((n_tp,)), dma((n_ep,)), dma((n_ep,)),
            dma((n_tp // 2, groups)), dma((n_tp // 2, groups)), dma((n_tp, groups)),
            dma((n_tp // 2, groups)), dma((n_tp // 2, groups)), dma((n_tp, groups)),
            dma((n_ep,)), dma((n_ep,)),
        ],
        compiler_params=pltpu.CompilerParams(
            collective_id=0, has_side_effects=True, vmem_limit_bytes=60 * 1024 * 1024),
    )(tokens, norm_gain[None, :], expert_ids.T, expert_weights.T, gate_weight, up_weight, down_weight)


def solution(mesh):
    in_specs = (
        P("ep", "tp"),
        P("tp"),
        P("ep", None),
        P("ep", None),
        P("ep", None, "tp"),
        P("ep", None, "tp"),
        P("ep", None, "tp"),
    )
    fn = functools.partial(body, mesh.shape["ep"], mesh.shape["tp"])
    return jax.shard_map(fn, mesh=mesh, in_specs=in_specs, out_specs=P("ep", "tp"), check_vma=False)
```

profile of v0, /device:TPU:13, one launch (start us, length us, event | category | flops | bytes accessed | tf_op | source)
XLA Modules:
  0.0 94.3 jit_solution(11270591558185092750)
XLA Ops:
  0.0 92.4 %shard_map.73 = bf16[256,1024]{1,0:T(8,128)(2,1)} custom-call(bf16[256,1024]{1,0:T(8,128)(2,1)} %tok.1, f32[1,1024]{1,0:T(1,128)} %bitcast.3, s32[2,256]{1,0:T(2,128)} %bitcast.4, f32[2,256]{1,0:T(2,128)} %bitcast.5, bf16[1,4096,512]{2,1,0:T(8,128)(2,1)} %gate_hbm.1, bf16[1,4096,512]{2,1,0:T(8,128)(2,1)} %up_hbm.1, bf16[1,2048,1024]{2,1,0:T(8,128)(2,1)} %down_hbm.1), custom_call_target="tpu_custom_call" | custom-call | tf_op jit(solution)/shard_map/pallas_call | solution.py:253
  92.4 1.9 %copy.9 = bf16[256,1024]{1,0:T(8,128)(2,1)} copy(bf16[256,1024]{1,0:T(8,128)(2,1)} %shard_map.73) | data formatting | bytes 1048576
where the time goes:
time: 94.4 us; the launch traced here: 94.3 us
  Pallas kernels  92.4 us (98%)
  local copies, waits for them, and re-layouts  1.87 us (2%)
    pallas_call x1, Pallas kernels, body(): pl.pallas_call(functools.partial(kernel, n_ep, n_tp, groups, cap), out_sh...  92.4 us

commit v1 on v0

v1 whole, which is shorter than its diff:
```python
import functools

import jax
import jax.numpy as jnp
from jax import lax
from jax.experimental import pallas as pl
from jax.experimental.pallas import tpu as pltpu
from jax.sharding import PartitionSpec as P

MESH = pl.DeviceIdType.MESH
F32 = jnp.float32
BF16 = jnp.bfloat16


INNER = (
    "s0", "t6", "a0", "o2", "o1", "o3", "a2", "b0", "c0", "r6", "p61", "p63", "p62", "q6", "a6",
    "b2", "c2", "d0", "e0", "f0", "a7", "b6", "c6", "d2", "r4", "p41", "p43", "p42", "q4", "e2",
    "a3", "b7", "c7", "d6", "e6", "f2", "a5", "b3", "c3", "d7", "f6", "e7", "f3", "a1", "b5",
    "c5", "d3", "e3", "a4", "b1", "f5", "c1", "d5", "f7", "e5", "f4", "b4", "c4", "d1", "e1",
    "d4", "e4", "f1",
)
OUTER = (
    "s0", "a0", "o2", "o3", "o1", "w4", "t4", "a2", "b0", "c0", "a3", "b2", "c2", "d0", "e0",
    "f0", "a5", "b3", "c3", "d2", "e2", "a4", "b5", "c5", "d3", "e3", "a7", "b4", "c4", "d5",
    "e5", "a6", "b7", "f2", "c7", "d4", "e4", "a1", "b6", "c6", "d7", "e7", "f3", "b1", "c1",
    "d6", "e6", "d1", "f7", "e1", "f5", "f6", "f1", "f4",
)

def kernel(
    n_ep, n_tp, groups, cap,
    tok, gain, ids, wts, gate_hbm, up_hbm, down_hbm,
    out,
    wg, wu, wd, squares_out, squares_in, key, weight, outgoing, rows, hid, prod, ret, acc,
    mine, raw, sums_out, far_ids, far_sums, far_key,
    w_sem, sq_send, sq_recv, d_send, d_recv, ry_send, rp_send, r_recv,
    hy_send, hp_send, h_recv, b_send, b_recv, f_send, f_recv,
):
    e = lax.axis_index("ep")
    t = lax.axis_index("tp")
    size = n_ep // groups
    block, place = e // size, e % size
    n_tok, width = tok.shape
    partner = t + 1 - 2 * (t % 2)
    pairs = n_tp // 2
    half = n_ep // 2
    relays = groups == 8
    inner = (block + 2) // 4 == 1

    loads = [
        pltpu.make_async_copy(gate_hbm.at[0], wg, w_sem.at[0]),
        pltpu.make_async_copy(up_hbm.at[0], wu, w_sem.at[1]),
        pltpu.make_async_copy(down_hbm.at[0], wd, w_sem.at[2]),
    ]

    barrier = pltpu.get_barrier_semaphore()
    for i in range(1, n_ep):
        pl.semaphore_signal(barrier, inc=1, device_id={"ep": (e + i) % n_ep}, device_id_type=MESH)
    for i in range(1, n_tp):
        pl.semaphore_signal(barrier, inc=1, device_id={"tp": (t + i) % n_tp}, device_id_type=MESH)
    for load in loads:
        load.start()

    def member(k, j):
        return (block ^ k) * size + (place + j) % size

    def far_copy(k, i):
        lane = 0 if k == 6 else 1
        src, dst = ((ids, far_ids), (tok, raw), (sums_out, far_sums))[i]
        return pltpu.make_async_remote_copy(
            src, dst.at[lane], f_send.at[i], f_recv.at[lane, i],
            device_id={"ep": member(k, 0)}, device_id_type=MESH)

    x = tok[...].astype(F32)
    part = jnp.sum(x * x, axis=1, keepdims=True)
    part = jnp.transpose(jnp.broadcast_to(part, (n_tok, 128)))[0:8]
    squares_out[...] = part
    pl.semaphore_wait(barrier, n_ep + n_tp - 2)

    def sq_copy(i, shard):
        return pltpu.make_async_remote_copy(
            squares_out, squares_in.at[shard], sq_send.at[i], sq_recv.at[shard],
            device_id={"tp": (t + i) % n_tp}, device_id_type=MESH)

    for i in range(1, n_tp):
        sq_copy(i, t).start()

    if relays:
        @pl.when(inner)
        def _():
            far_copy(6, 0).start()
            far_copy(6, 1).start()

    experts = key.shape[0]

    def named_slots(ids):
        which = lax.broadcasted_iota(jnp.int32, (experts, n_tok), 0)
        first, second = ids[0:1, :] == which, ids[1:2, :] == which
        named = jnp.where(first | second, 1.0, 0.0)
        before = lax.broadcasted_iota(jnp.int32, (n_tok, n_tok), 0) < lax.broadcasted_iota(
            jnp.int32, (n_tok, n_tok), 1)
        rank = jnp.dot(named.astype(BF16), jnp.where(before, 1.0, 0.0).astype(BF16),
                       preferred_element_type=F32)
        return first, second, jnp.where(first | second, rank, -1.0)

    first, second, slot = named_slots(ids)
    share = jnp.where(first, wts[0:1, :], 0.0) + jnp.where(second, wts[1:2, :], 0.0)
    for d in range(experts):
        key[d] = jnp.broadcast_to(slot[d:d + 1], (8, n_tok))
        weight[d] = jnp.broadcast_to(share[d:d + 1], (8, n_tok))

    def chosen(row, value):
        number = (lax.broadcasted_iota(jnp.int32, (cap // 8, 8, n_tok), 0) * 8
                  + lax.broadcasted_iota(jnp.int32, (cap // 8, 8, n_tok), 1)).astype(F32)
        return jnp.where(number == row[None], value, 0.0).reshape(cap, n_tok)

    def normalized(values, total):
        inv = lax.rsqrt(total / (width * n_tp) + 1e-06)
        inv = jnp.transpose(jnp.broadcast_to(inv[0:1], (128, n_tok)))[:, 0:1]
        return (values.astype(F32) * inv * gain[...]).astype(BF16)

    total = part
    for i in range(1, n_tp):
        other = (t + i) % n_tp
        sq_copy(i, other).wait_recv()
        total = total + squares_in[other]
    sums_out[...] = total
    mine[...] = normalized(tok[...], total)

    def dispatch(slot, d, s):
        return pltpu.make_async_remote_copy(
            outgoing.at[slot], rows.at[t, s], d_send.at[slot], d_recv.at[s],
            device_id={"ep": d}, device_id_type=MESH)

    def back(s, d):
        return pltpu.make_async_remote_copy(
            prod.at[s], ret.at[d], b_send.at[s], b_recv.at[d],
            device_id={"ep": s}, device_id_type=MESH)

    def peers(k):
        return range(1 if k == 0 else 0, size)

    def picked(row, values):
        return jnp.dot(chosen(row, 1.0).astype(BF16), values[...],
                       preferred_element_type=F32).astype(BF16)

    def span(k):
        return pl.ds((block ^ k) * size, size)

    def across(buf, k, i, shard, send, recv):
        ref = buf.at[shard, span(k)]
        return pltpu.make_async_remote_copy(
            ref, ref, send.at[i, k], recv.at[shard, k],
            device_id={"tp": (t + 2 * i) % n_tp}, device_id_type=MESH)

    def beside(buf, k, i, shard, send, recv):
        ref = buf.at[shard, span(k)]
        return pltpu.make_async_remote_copy(
            ref, ref, send.at[i, k], recv.at[shard, k],
            device_id={"tp": partner}, device_id_type=MESH)

    def spread(buf, k, ysend, psend, recv):
        for i in range(1, pairs):
            across(buf, k, i, t, ysend, recv).start()
        beside(buf, k, 0, t, psend, recv).start()

    def pass_on(buf, k, ysend, psend, recv):
        for i in range(1, pairs):
            shard = (t + n_tp - 2 * i) % n_tp
            across(buf, k, i, shard, ysend, recv).wait_recv()
            beside(buf, k, i, shard, psend, recv).start()

    def complete(buf, k, psend, recv):
        for i in range(pairs):
            shard = (partner + n_tp - 2 * i) % n_tp
            beside(buf, k, i, shard, psend, recv).wait_recv()

    row_sems, hid_sems = (ry_send, rp_send, r_recv), (hy_send, hp_send, h_recv)

    def own_slot(k, d):
        return d % half + (half if k >= groups // 2 else 0)

    def far_slot(lane, d):
        return d % half + half * (1 + lane)

    def run(program):
        relayed = [k for name, k in program if name == "r"]
        combined = [k for name, k in program if name == "f"]
        loaded = []

        def need(*which):
            for i in which:
                if i not in loaded:
                    loads[i].wait()
                    loaded.append(i)

        def stage_s(k):
            rows[t, e] = picked(key[e], mine)

        def stage_o(k):
            for j in peers(k):
                d = member(k, j)
                outgoing[own_slot(k, d)] = picked(key[d], mine)
                dispatch(own_slot(k, d), d, e).start()

        def stage_t(k):
            far_copy(k, 2).start()

        def stage_w(k):
            far_copy(k, 0).start()
            far_copy(k, 1).start()

        def stage_r(k):
            lane = 0 if k == 6 else 1
            for i in range(3):
                far_copy(k, i).wait_recv()
            far = named_slots(far_ids[lane])[2]
            for d in range(experts):
                far_key[lane, d] = jnp.broadcast_to(far[d:d + 1], (8, n_tok))
            raw[lane] = normalized(raw[lane], far_sums[lane])

        def stage_p(k):
            lane, k = (0, k - 60) if k >= 60 else (1, k - 40)
            source = member((6, 4)[lane], 0)
            for j in peers(k):
                d = member(k, j)
                outgoing[far_slot(lane, d)] = picked(far_key[lane, d], raw.at[lane])
                dispatch(far_slot(lane, d), d, source).start()

        def stage_q(k):
            lane = 0 if k == 6 else 1
            rows[t, member(k, 0)] = picked(far_key[lane, e], raw.at[lane])

        def stage_a(k):
            local = k == 0 or k in relayed
            for j in range(1 if local else 0, size):
                s = member(k, j)
                dispatch(s, s, s).wait_recv()
            spread(rows, k, *row_sems)

        def stage_b(k):
            pass_on(rows, k, *row_sems)

        def stage_c(k):
            complete(rows, k, rp_send, r_recv)
            need(0, 1)
            gate = up = None
            for shard in range(n_tp):
                part_rows = rows[shard, span(k)].reshape(size * cap, width)
                g = jnp.dot(part_rows, wg[shard * width:(shard + 1) * width, :],
                            preferred_element_type=F32)
                u = jnp.dot(part_rows, wu[shard * width:(shard + 1) * width, :],
                            preferred_element_type=F32)
                gate, up = (g, u) if gate is None else (gate + g, up + u)
            hidden = (gate / (1.0 + jnp.exp(-gate)) * up).astype(BF16)
            hid[t, span(k)] = hidden.reshape(size, cap, hidden.shape[1])
            spread(hid, k, *hid_sems)

        def stage_d(k):
            pass_on(hid, k, *hid_sems)

        def stage_e(k):
            complete(hid, k, hp_send, h_recv)
            need(2)
            units = hid.shape[3]
            made = None
            for shard in range(n_tp):
                m = jnp.dot(hid[shard, span(k)].reshape(size * cap, units),
                            wd[shard * units:(shard + 1) * units, :], preferred_element_type=F32)
                made = m if made is None else made + m
            prod[span(k)] = made.astype(BF16).reshape(size, cap, width)
            for j in peers(k):
                back(member(k, j), e).start()
            if k == 0:
                ret[e] = prod[e]

        def stage_f(k):
            for j in peers(k):
                d = member(k, j)
                back(d, d).wait_recv()
            base = (block ^ k) * size
            tables = jnp.concatenate(
                [chosen(key[base + j], weight[base + j][None]) for j in range(size)], axis=0)
            high = tables.astype(BF16)
            low = (tables - high.astype(F32)).astype(BF16)
            values = ret[span(k)].reshape(size * cap, width)
            dims = (((0,), (0,)), ((), ()))
            sums = lax.dot_general(high, values, dims, preferred_element_type=F32)
            sums = sums + lax.dot_general(low, values, dims, preferred_element_type=F32)
            if k != combined[0]:
                sums = sums + acc[...]
            if k != combined[-1]:
                acc[...] = sums
            else:
                out[...] = sums.astype(BF16)

        stages = dict(
            s=stage_s, o=stage_o, t=stage_t, w=stage_w, r=stage_r, p=stage_p, q=stage_q,
            a=stage_a, b=stage_b, c=stage_c, d=stage_d, e=stage_e, f=stage_f)
        for name, k in program:
            stages[name](k)

        for name, k in program:
            if name == "o":
                for j in peers(k):
                    d = member(k, j)
                    dispatch(own_slot(k, d), d, e).wait_send()
            if name == "p":
                lane, to = (0, k - 60) if k >= 60 else (1, k - 40)
                for j in peers(to):
                    d = member(to, j)
                    dispatch(far_slot(lane, d), d, e).wait_send()
            if name == "t":
                for i in range(3):
                    far_copy(k, i).wait_send()

    def steps(text):
        return [(item[0], int(item[1:])) for item in text]

    if relays:
        @pl.when(inner)
        def _():
            run(steps(INNER))

        @pl.when(jnp.logical_not(inner))
        def _():
            run(steps(OUTER))
    else:
        order = [("s", 0)] + [("o", k) for k in range(groups)]
        for k in range(groups):
            order += [(name, k) for name in "abcde"]
        run(order + [("f", k) for k in range(groups)])

    for i in range(1, n_tp):
        sq_copy(i, t).wait_send()
    for k in range(groups):
        for j in peers(k):
            back(member(k, j), e).wait_send()
        for buf, ysend, psend, recv in ((rows,) + row_sems, (hid,) + hid_sems):
            for i in range(pairs):
                if i > 0:
                    across(buf, k, i, t, ysend, recv).wait_send()
                beside(buf, k, i, t, psend, recv).wait_send()


def body(n_ep, n_tp, tokens, norm_gain, expert_ids, expert_weights, gate_weight, up_weight, down_weight):
    n_tok, width = tokens.shape
    experts = gate_weight.shape[0] * n_ep
    cap = 3 * n_tok * expert_ids.shape[1] // (2 * experts)
    depth, units = gate_weight.shape[1:]
    hidden = down_weight.shape[1]
    groups = next(g for g in (8, 4, 2, 1) if n_ep % g == 0)
    vmem = pl.BlockSpec(memory_space=pltpu.VMEM)
    hbm = pl.BlockSpec(memory_space=pl.ANY)
    dma = pltpu.SemaphoreType.DMA
    return pl.pallas_call(
        functools.partial(kernel, n_ep, n_tp, groups, cap),
        out_shape=jax.ShapeDtypeStruct((n_tok, width), BF16),
        in_specs=[vmem] * 4 + [hbm] * 3,
        out_specs=vmem,
        scratch_shapes=[
            pltpu.VMEM((depth, units), BF16),
            pltpu.VMEM((depth, units), BF16),
            pltpu.VMEM((hidden, width), BF16),
            pltpu.VMEM((8, n_tok), F32),
            pltpu.VMEM((n_tp, 8, n_tok), F32),
            pltpu.VMEM((experts, 8, n_tok), F32),
            pltpu.VMEM((experts, 8, n_tok), F32),
            pltpu.VMEM((2 * n_ep, cap, width), BF16),
            pltpu.VMEM((n_tp, n_ep, cap, width), BF16),
            pltpu.VMEM((n_tp, n_ep, cap, units), BF16),
            pltpu.VMEM((n_ep, cap, width), BF16),
            pltpu.VMEM((n_ep, cap, width), BF16),
            pltpu.VMEM((n_tok, width), F32),
            pltpu.VMEM((n_tok, width), BF16),
            pltpu.VMEM((2, n_tok, width), BF16),
            pltpu.VMEM((8, n_tok), F32),
            pltpu.VMEM((2, 2, n_tok), jnp.int32),
            pltpu.VMEM((2, 8, n_tok), F32),
            pltpu.VMEM((2, experts, 8, n_tok), F32),
            dma((3,)), dma((n_tp,)), dma((n_tp,)), dma((2 * n_ep,)), dma((n_ep,)),
            dma((n_tp // 2, groups)), dma((n_tp // 2, groups)), dma((n_tp, groups)),
            dma((n_tp // 2, groups)), dma((n_tp // 2, groups)), dma((n_tp, groups)),
            dma((n_ep,)), dma((n_ep,)), dma((3,)), dma((2, 3)),
        ],
        compiler_params=pltpu.CompilerParams(
            collective_id=0, has_side_effects=True, vmem_limit_bytes=60 * 1024 * 1024),
    )(tokens, norm_gain[None, :], expert_ids.T, expert_weights.T, gate_weight, up_weight, down_weight)


def solution(mesh):
    in_specs = (
        P("ep", "tp"),
        P("tp"),
        P("ep", None),
        P("ep", None),
        P("ep", None, "tp"),
        P("ep", None, "tp"),
        P("ep", None, "tp"),
    )
    fn = functools.partial(body, mesh.shape["ep"], mesh.shape["tp"])
    return jax.shard_map(fn, mesh=mesh, in_specs=in_specs, out_specs=P("ep", "tp"), check_vma=False)
```

time: 94.4 us -> 83.9 us (0.89); the launches traced: 94.3 us -> 82.4 us
  Pallas kernels: 92.4 us -> 80.5 us
    pallas_call x1, Pallas kernels: 92.4 us -> 80.5 us  [body(): pl.pallas_call(functools.partial(kernel, n_ep, n_tp, groups, cap), out_sh...]
where the time goes in v1:
time: 83.9 us; the launch traced here: 82.4 us
  Pallas kernels  80.5 us (96%)
  local copies, waits for them, and re-layouts  1.87 us (2%)
    pallas_call x1, Pallas kernels, body(): pl.pallas_call(functools.partial(kernel, n_ep, n_tp, groups, cap), out_sh...  80.5 us
    unnamed x1, local copies, waits for them, and re-layouts  1.87 us

profile of v1, /device:TPU:13, one launch (start us, length us, event | category | flops | bytes accessed | tf_op | source)
XLA Modules:
  0.0 82.4 jit_solution(4570645644235444606)
XLA Ops:
  0.0 80.5 %shard_map.73 = bf16[256,1024]{1,0:T(8,128)(2,1)} custom-call(bf16[256,1024]{1,0:T(8,128)(2,1)} %tok.1, f32[1,1024]{1,0:T(1,128)} %bitcast.3, s32[2,256]{1,0:T(2,128)} %bitcast.4, f32[2,256]{1,0:T(2,128)} %bitcast.5, bf16[1,4096,512]{2,1,0:T(8,128)(2,1)} %gate_hbm.1, bf16[1,4096,512]{2,1,0:T(8,128)(2,1)} %up_hbm.1, bf16[1,2048,1024]{2,1,0:T(8,128)(2,1)} %down_hbm.1), custom_call_target="tpu_custom_call" | custom-call | tf_op jit(solution)/shard_map/pallas_call | solution.py:355
  80.5 1.9 %copy.9 = bf16[256,1024]{1,0:T(8,128)(2,1)} copy(bf16[256,1024]{1,0:T(8,128)(2,1)} %shard_map.73) | data formatting | bytes 1048576

commit v2 on v1

--- a/solution.py
+++ b/solution.py
@@ -28,10 +28,10 @@
 
 def kernel(
     n_ep, n_tp, groups, cap,
-    tok, gain, ids, wts, gate_hbm, up_hbm, down_hbm,
+    tok_hbm, gain, ids, wts, gate_hbm, up_hbm, down_hbm,
     out,
     wg, wu, wd, squares_out, squares_in, key, weight, outgoing, rows, hid, prod, ret, acc,
-    mine, raw, sums_out, far_ids, far_sums, far_key,
+    mine, raw, sums_out, far_ids, far_sums, far_key, tok, gates, ups, mades,
     w_sem, sq_send, sq_recv, d_send, d_recv, ry_send, rp_send, r_recv,
     hy_send, hp_send, h_recv, b_send, b_recv, f_send, f_recv,
 ):
@@ -51,6 +51,8 @@
         pltpu.make_async_copy(up_hbm.at[0], wu, w_sem.at[1]),
         pltpu.make_async_copy(down_hbm.at[0], wd, w_sem.at[2]),
     ]
+    fetch = pltpu.make_async_copy(tok_hbm, tok, w_sem.at[3])
+    fetch.start()
 
     barrier = pltpu.get_barrier_semaphore()
     for i in range(1, n_ep):
@@ -70,6 +72,7 @@
             src, dst.at[lane], f_send.at[i], f_recv.at[lane, i],
             device_id={"ep": member(k, 0)}, device_id_type=MESH)
 
+    fetch.wait()
     x = tok[...].astype(F32)
     part = jnp.sum(x * x, axis=1, keepdims=True)
     part = jnp.transpose(jnp.broadcast_to(part, (n_tok, 128)))[0:8]
@@ -169,11 +172,6 @@
             across(buf, k, i, shard, ysend, recv).wait_recv()
             beside(buf, k, i, shard, psend, recv).start()
 
-    def complete(buf, k, psend, recv):
-        for i in range(pairs):
-            shard = (partner + n_tp - 2 * i) % n_tp
-            beside(buf, k, i, shard, psend, recv).wait_recv()
-
     row_sems, hid_sems = (ry_send, rp_send, r_recv), (hy_send, hp_send, h_recv)
 
     def own_slot(k, d):
@@ -237,36 +235,55 @@
                 dispatch(s, s, s).wait_recv()
             spread(rows, k, *row_sems)
 
+        def shard_of(buf, k, n, psend, recv):
+            if n is None or isinstance(n, int):
+                n = n or 0
+                shard = (partner + n_tp - 2 * n) % n_tp
+                beside(buf, k, n, shard, psend, recv).wait_recv()
+                return shard
+            return n
+
+        def taken(weights, shard, depth):
+            return weights[pl.ds(pl.multiple_of(shard * depth, depth), depth), :]
+
+        def gate_up(k, shards, gate=None, up=None):
+            for n in shards:
+                shard = shard_of(rows, k, n, rp_send, r_recv)
+                part_rows = rows[shard, span(k)].reshape(size * cap, width)
+                g = jnp.dot(part_rows, taken(wg, shard, width), preferred_element_type=F32)
+                u = jnp.dot(part_rows, taken(wu, shard, width), preferred_element_type=F32)
+                gate, up = (g, u) if gate is None else (gate + g, up + u)
+            return gate, up
+
+        def down(k, shards, made=None):
+            units = hid.shape[3]
+            for n in shards:
+                shard = shard_of(hid, k, n, hp_send, h_recv)
+                values = hid[shard, span(k)].reshape(size * cap, units)
+                m = jnp.dot(values, taken(wd, shard, units), preferred_element_type=F32)
+                made = m if made is None else made + m
+            return made
+
         def stage_b(k):
             pass_on(rows, k, *row_sems)
+            need(0, 1)
+            near = [(t + n_tp - 2 * i) % n_tp for i in range(pairs)]
+            gates[k], ups[k] = gate_up(k, near[:1] + [None] + near[1:])
 
         def stage_c(k):
-            complete(rows, k, rp_send, r_recv)
-            need(0, 1)
-            gate = up = None
-            for shard in range(n_tp):
-                part_rows = rows[shard, span(k)].reshape(size * cap, width)
-                g = jnp.dot(part_rows, wg[shard * width:(shard + 1) * width, :],
-                            preferred_element_type=F32)
-                u = jnp.dot(part_rows, wu[shard * width:(shard + 1) * width, :],
-                            preferred_element_type=F32)
-                gate, up = (g, u) if gate is None else (gate + g, up + u)
+            gate, up = gate_up(k, range(1, pairs), gates[k], ups[k])
             hidden = (gate / (1.0 + jnp.exp(-gate)) * up).astype(BF16)
             hid[t, span(k)] = hidden.reshape(size, cap, hidden.shape[1])
             spread(hid, k, *hid_sems)
 
         def stage_d(k):
             pass_on(hid, k, *hid_sems)
+            need(2)
+            near = [(t + n_tp - 2 * i) % n_tp for i in range(pairs)]
+            mades[k] = down(k, near[:1] + [None] + near[1:])
 
         def stage_e(k):
-            complete(hid, k, hp_send, h_recv)
-            need(2)
-            units = hid.shape[3]
-            made = None
-            for shard in range(n_tp):
-                m = jnp.dot(hid[shard, span(k)].reshape(size * cap, units),
-                            wd[shard * units:(shard + 1) * units, :], preferred_element_type=F32)
-                made = m if made is None else made + m
+            made = down(k, range(1, pairs), mades[k])
             prod[span(k)] = made.astype(BF16).reshape(size, cap, width)
             for j in peers(k):
                 back(member(k, j), e).start()
@@ -354,8 +371,8 @@
     dma = pltpu.SemaphoreType.DMA
     return pl.pallas_call(
         functools.partial(kernel, n_ep, n_tp, groups, cap),
-        out_shape=jax.ShapeDtypeStruct((n_tok, width), BF16),
-        in_specs=[vmem] * 4 + [hbm] * 3,
+        out_shape=pltpu.VMEM((n_tok, width), BF16),
+        in_specs=[hbm] + [vmem] * 3 + [hbm] * 3,
         out_specs=vmem,
         scratch_shapes=[
             pltpu.VMEM((depth, units), BF16),
@@ -377,7 +394,11 @@
             pltpu.VMEM((2, 2, n_tok), jnp.int32),
             pltpu.VMEM((2, 8, n_tok), F32),
             pltpu.VMEM((2, experts, 8, n_tok), F32),
-            dma((3,)), dma((n_tp,)), dma((n_tp,)), dma((2 * n_ep,)), dma((n_ep,)),
+            pltpu.VMEM((n_tok, width), BF16),
+            pltpu.VMEM((groups, n_ep // groups * cap, units), F32),
+            pltpu.VMEM((groups, n_ep // groups * cap, units), F32),
+            pltpu.VMEM((groups, n_ep // groups * cap, width), F32),
+            dma((4,)), dma((n_tp,)), dma((n_tp,)), dma((2 * n_ep,)), dma((n_ep,)),
             dma((n_tp // 2, groups)), dma((n_tp // 2, groups)), dma((n_tp, groups)),
             dma((n_tp // 2, groups)), dma((n_tp // 2, groups)), dma((n_tp, groups)),
             dma((n_ep,)), dma((n_ep,)), dma((3,)), dma((2, 3)),

time: 83.9 us -> 81.1 us (0.967)
  the two profiles are of different devices: /device:TPU:13 before, /device:TPU:0 now
where the time goes in v2:
time: 81.1 us; the launch traced here: 80.9 us
  Pallas kernels  80.1 us (99%)
    pallas_call x1, Pallas kernels, body(): pl.pallas_call(functools.partial(kernel, n_ep, n_tp, groups, cap), out_sh...  80.1 us

profile of v2, /device:TPU:0, one launch (start us, length us, event | category | flops | bytes accessed | tf_op | source)
XLA Modules:
  0.0 80.9 jit_solution(15173410219818919267)
XLA Ops:
  0.0 80.1 %shard_map.73 = bf16[256,1024]{1,0:T(8,128)(2,1)S(1)} custom-call(bf16[256,1024]{1,0:T(8,128)(2,1)} %tok_hbm.1, f32[1,1024]{1,0:T(1,128)} %bitcast.3, s32[2,256]{1,0:T(2,128)} %bitcast.4, f32[2,256]{1,0:T(2,128)} %bitcast.5, bf16[1,4096,512]{2,1,0:T(8,128)(2,1)} %gate_hbm.1, bf16[1,4096,512]{2,1,0:T(8,128)(2,1)} %up_hbm.1, bf16[1,2048,1024]{2,1,0:T(8,128)(2,1)} %down_hbm.1), custom_call_target="tpu_custom_call" | custom-call | tf_op jit(solution)/shard_map/pallas_call | solution.py:372
  80.1 0.8 copy.9
